TPU v7x, 32 devices: a whole 2x2x4 slice. The times are simulated.
32 devices in a mesh: grp: 2 (over x), tp: 16 (over z, y, core).
Axes of the slice: x: 2, y: 2, z: 4, core: 2. Of those that a mesh axis runs over, the one named last changes fastest.
Arguments:
- tokens: bfloat16 [160, 2048], P('grp', 'tp'), parts along dimension 0, may hold values from -6 to 6
- lengths: int32 [160], P('grp'), parts along dimension 0, may hold values from 1 to 4096, 81920 in all
- cell_memory: float32 [2, 160, 2048, 256], P(None, 'grp', 'tp'), parts along dimension 1, may hold values from -0.6 to 0.6
- key_sums: float32 [2, 160, 2048], P(None, 'grp', 'tp'), parts along dimension 1, may hold values from -3 to 3
- stabilizer: float32 [2, 160, 8], P(None, 'grp'), parts along dimension 1, may hold values from -3 to 1
- norm_gain: bfloat16 [2, 2048], replicated, may hold values from 0.099609375 to 1.8984375
- query_weight: bfloat16 [2, 2048, 2048], P(None, None, 'tp'), may hold values from -0.125 to 0.125
- key_weight: bfloat16 [2, 2048, 2048], P(None, None, 'tp'), may hold values from -0.125 to 0.125
- value_weight: bfloat16 [2, 2048, 2048], P(None, None, 'tp'), may hold values from -0.125 to 0.125
- outgate_weight: bfloat16 [2, 2048, 2048], P(None, None, 'tp'), may hold values from -0.125 to 0.125
- ingate_weight: bfloat16 [2, 2048, 8], replicated, may hold values from -0.125 to 0.125
- forget_weight: bfloat16 [2, 2048, 8], replicated, may hold values from -0.125 to 0.125
- ingate_bias: float32 [2, 8], replicated, may hold values from -3 to 3
- forget_bias: float32 [2, 8], replicated, may hold values from -1 to 4
- forget_slope: float32 [2, 8], replicated, may hold values from -3 to 3
- head_gain: bfloat16 [2, 2048], P(None, 'tp'), may hold values from 0.099609375 to 1.8984375
- output_weight: bfloat16 [2, 2048, 2048], P(None, None, 'tp'), may hold values from -0.125 to 0.125
Outputs:
- new_tokens: bfloat16 [160, 2048], P('grp', 'tp'), parts along dimension 0
- new_memory: float32 [2, 160, 2048, 256], P(None, 'grp', 'tp'), parts along dimension 1
- new_key_sums: float32 [2, 160, 2048], P(None, 'grp', 'tp'), parts along dimension 1
- new_stabilizer: float32 [2, 160, 8], P(None, 'grp'), parts along dimension 1
There are 2 independent parts, one for each index of `grp`. A program takes and returns all parts, laid end to end along the dimension named above; an argument that names none is the same for every part. Nothing has to cross between parts.
Inputs may be any that keep to these rules, and one draw needn't show every extreme that they name: Each part's 80 lengths sum to 81920, and the largest is exactly 4096.
All inputs are finite; a program needn't handle non-finite values.
Results may differ from a plain program's by a relative error of at most 0.018.
Values may be sent and summed in bfloat16 or wider, within the bound.
A program may use at most 128 MiB of HBM per device.

v0:
```python
import functools

import jax
import jax.numpy as jnp
from jax import lax
from jax.experimental import pallas as pl
from jax.experimental.pallas import tpu as pltpu
from jax.sharding import PartitionSpec as P

HEADS = 8
HEAD = 256
MAXLEN = 4096
EPS = 1e-05
MESH = pl.DeviceIdType.MESH
F32 = jnp.float32
BF16 = jnp.bfloat16
GROUP = 8


def parts_of(batch):
    first = (batch + 31) // 32 * 16
    return ((0, first), (first, batch - first))


def kernel(
    n,
    tokens,
    lengths,
    cell_memory,
    key_sums,
    stabilizer,
    norm_gain,
    query_weight,
    key_weight,
    value_weight,
    outgate_weight,
    ingate_weight,
    forget_weight,
    ingate_bias,
    forget_bias,
    forget_slope,
    head_gain,
    output_weight,
    new_tokens,
    mem,
    new_sums,
    new_stab,
    lengths_in,
    stabilizer_in,
    norm_gain_in,
    ingate_bias_in,
    forget_bias_in,
    forget_slope_in,
    head_gain_in,
    wbig,
    wout,
    wgi,
    wgate,
    small_sem,
    gath,
    sums,
    vt_ref,
    decay_ref,
    kk_ref,
    local_sem,
    mem_sem,
    gsend,
    gfwd,
    grecv,
    wsend,
    wrecv,
    ssend,
    srecv,
):
    blocks, batch, rows, head = mem.shape
    heads = stabilizer.shape[1]
    width = output_weight.shape[1]
    split = n // heads
    chips = n // 2
    me = lax.axis_index("tp")
    chip = me // 2
    core = lax.rem(me, 2)
    sibling = me + 1 - 2 * core
    own_head = me // split
    lanes = pl.multiple_of
    parts = parts_of(batch)

    half, quarter = chips // 2, chips // 4
    flip = chip // half
    seat = chip + flip * (chips - 1 - 2 * chip)

    def unflip(d):
        return d + flip * (chips - 1 - 2 * d)

    far_chips = [unflip(chips - 1 - i) for i in range(half)]
    near_chips = [unflip(lax.rem(seat + i, half)) for i in range(1, half)]
    far_group = 2 - seat // quarter
    targets = [(c, far_group) for c in far_chips] + [(c, 0) for c in near_chips]
    groups = (
        near_chips,
        [unflip(half + i) for i in range(quarter)],
        [unflip(half + quarter + i) for i in range(quarter)],
    )

    own_copy = pltpu.make_async_copy(tokens, gath.at[0, me], local_sem.at[0, 3])
    own_copy.start()
    sums_copy = pltpu.make_async_copy(key_sums, sums.at[core], local_sem.at[1, 3])
    small = [
        pltpu.make_async_copy(a, b, small_sem.at[i])
        for i, (a, b) in enumerate(
            (
                (lengths, lengths_in),
                (stabilizer, stabilizer_in),
                (norm_gain, norm_gain_in),
                (ingate_bias, ingate_bias_in),
                (forget_bias, forget_bias_in),
                (forget_slope, forget_slope_in),
                (head_gain, head_gain_in),
            )
        )
    ]
    own_query = pl.ds(lanes(core * rows, rows), rows)
    own_key = pl.ds(lanes(head + core * rows, rows), rows)
    places = (own_query, own_key, pl.ds(2 * head, rows), pl.ds(2 * head + rows, rows))

    def load(l):
        for i, w in enumerate((query_weight, key_weight, value_weight, outgate_weight)):
            pltpu.make_async_copy(w.at[l], wbig.at[l, :, places[i]], local_sem.at[l, 0]).start()
        pltpu.make_async_copy(ingate_weight.at[l], wgi.at[l, 0], local_sem.at[l, 1]).start()
        pltpu.make_async_copy(forget_weight.at[l], wgi.at[l, 1], local_sem.at[l, 1]).start()
        if l == 0:
            for c in small:
                c.start()
            sums_copy.start()
        own = wout.at[l, :, pl.ds(lanes(core * rows, rows), rows)]
        pltpu.make_async_copy(output_weight.at[l], own, local_sem.at[l, 2]).start()
        pltpu.make_async_copy(cell_memory.at[l], mem.at[l], mem_sem.at[l]).start()

    def loaded(ref, sem):
        pltpu.make_async_copy(ref, ref, sem).wait()

    load(0)

    barrier = pltpu.get_barrier_semaphore()
    pl.semaphore_signal(barrier, inc=1, device_id={"tp": sibling}, device_id_type=MESH)

    @pl.when(core == 1)
    def _():
        for c, _ in targets:
            for other in range(2):
                pl.semaphore_signal(
                    barrier, inc=1, device_id={"tp": c * 2 + other}, device_id_type=MESH
                )

    pl.semaphore_wait(barrier, chips)

    def remote(ref, send, recv, dest):
        return pltpu.make_async_remote_copy(
            src_ref=ref,
            dst_ref=ref,
            send_sem=send,
            recv_sem=recv,
            device_id={"tp": dest},
            device_id_type=MESH,
        )

    def block_copy(g, p, slot, group, send, dest):
        return remote(gath.at[g, slot, pl.ds(*parts[p])], send, grecv.at[g, p, group], dest)

    def pair_copy(g, p, c, group, send, dest):
        ref = gath.at[g, pl.ds(2 * c, 2), pl.ds(*parts[p])]
        return remote(ref, send, grecv.at[g, p, group], dest)

    def arrived(g, p, group, count):
        ref = gath.at[g, pl.ds(0, count), pl.ds(*parts[p])]
        remote(ref, gsend.at[g], grecv.at[g, p, group], sibling).wait_recv()

    def flushed(ref, sem):
        remote(ref, sem, wrecv.at[0, 0], sibling).wait_send()

    def send_own(g, p):
        for c, group in targets:
            block_copy(g, p, me, group, gsend.at[g], c * 2 + 1).start()

    def gathered(l, k):
        g = 2 * l
        if k < 0:
            for p in range(len(parts)):
                if l == 0:
                    arrived(g, p, 3, 1)
                else:

                    @pl.when(core == 0)
                    def _():
                        arrived(g, p, 3, 2)

            return [chip]
        for p in range(len(parts)):
            arrived(g, p, k, 2 * len(groups[k]))

            @pl.when(core == 1)
            def _():
                for c in groups[k]:
                    pair_copy(g, p, c, k, gfwd.at[l], sibling).start()

        return groups[k]

    own_copy.wait()
    for p in range(len(parts)):
        block_copy(0, p, me, 3, gsend.at[0], sibling).start()
        send_own(0, p)
    sums_copy.wait()
    sums_send = remote(sums.at[core], ssend, srecv, sibling)
    sums_send.start()

    def push_weights(l):
        loaded(wbig.at[l, :, pl.ds(0, 4 * rows)], local_sem.at[l, 0])
        for place in (own_query, own_key):
            remote(wbig.at[l, :, place], wsend.at[l, 0], wrecv.at[l, 0], sibling).start()
        loaded(wout.at[l, :, pl.ds(0, rows)], local_sem.at[l, 2])

        @pl.when(core == 0)
        def _():
            ref = wout.at[l, :, pl.ds(0, rows)]
            remote(ref, wsend.at[l, 1], wrecv.at[l, 1], sibling).start()

    push_weights(0)
    for l in range(1, blocks):
        load(l)
    for c in small:
        c.wait()
    eye = lax.broadcasted_iota(jnp.int32, (batch, batch), 0) == lax.broadcasted_iota(
        jnp.int32, (batch, batch), 1
    )
    position = jnp.sum(
        jnp.where(eye, lengths_in[...].astype(F32) / MAXLEN, 0.0), axis=1, keepdims=True
    )
    lane = lax.broadcasted_iota(jnp.int32, (rows, rows), 1)
    head_mask = lax.broadcasted_iota(jnp.int32, (batch, heads), 1) == own_head

    def project(l):
        old_stab = stabilizer_in[l].T
        bias = forget_bias_in[l : l + 1, :] + forget_slope_in[l : l + 1, :] * position

        def step(c, total):
            at = pl.ds(lanes(c * 2 * rows, 2 * rows), 2 * rows)
            x = jnp.concatenate((gath[2 * l, 2 * c], gath[2 * l, 2 * c + 1]), axis=1).astype(F32)
            gain = norm_gain_in[:, at].astype(F32)[l : l + 1]
            scaled = (x * gain).astype(BF16)
            part = jnp.dot(scaled, wbig[l, at, :], preferred_element_type=F32)
            gpart = lax.dot_general(
                scaled, wgate[l, :, at], (((1,), (1,)), ((), ())), preferred_element_type=F32
            )
            square = x * x
            if total is None:
                return part, gpart, square
            return total[0] + part, total[1] + gpart, total[2] + square

        total = None
        for k in range(-1, len(groups)):
            for c in gathered(l, k):
                total = step(c, total)
        proj, gates, square = total
        scale = lax.rsqrt(jnp.sum(square, axis=1, keepdims=True) / width + EPS)
        proj = proj * scale
        head_query = proj[:, :head].astype(BF16)
        head_key = (proj[:, head : 2 * head] * head ** (-0.5)).astype(BF16).astype(F32)
        value = proj[:, 2 * head : 2 * head + rows].astype(BF16).astype(F32)
        outgate = proj[:, 2 * head + rows :].astype(BF16).astype(F32)
        gates = gates * scale
        ingate = gates[:, :heads] + ingate_bias_in[l : l + 1, :]
        logit = gates[:, heads : 2 * heads] + bias
        forget = jnp.minimum(logit, 0.0) - jnp.log1p(jnp.exp(-jnp.abs(logit)))
        shifted = forget + old_stab
        stab = jnp.maximum(shifted, ingate)
        decay = jnp.sum(jnp.where(head_mask, jnp.exp(shifted - stab), 0.0), axis=1, keepdims=True)
        inweight = jnp.sum(
            jnp.where(head_mask, jnp.exp(ingate - stab), 0.0), axis=1, keepdims=True
        )
        gate = head_gain_in[...].astype(F32)[l : l + 1] * jax.nn.sigmoid(outgate)
        query_float = head_query.astype(F32)
        key_dot = jnp.sum(head_key * query_float, axis=1, keepdims=True)
        old = jnp.concatenate((sums[0, l], sums[1, l]), axis=1)
        sum_dot = jnp.sum(old * query_float, axis=1, keepdims=True)
        denominator = jnp.maximum(jnp.abs(decay * sum_dot + inweight * key_dot), 1.0)
        padded = jnp.concatenate((head_query, jnp.zeros((rows - batch, head), BF16)), axis=0)
        factor = gate / denominator
        return padded, decay * factor, inweight * key_dot * value * factor, (
            stab,
            decay,
            inweight,
            head_key,
            value,
        )

    def keep(l, held):
        stab, decay, inweight, head_key, value = held
        keyrow = jnp.where(core == 0, head_key[:, :rows], head_key[:, rows:])
        new_sums[l] = decay * sums[core, l] + inweight * keyrow
        new_stab[l] = stab.T
        vt_ref[...] = jnp.concatenate((value, jnp.zeros((rows - batch, rows), F32)), axis=0).T
        decay_ref[...] = jnp.broadcast_to(decay, (batch, head))
        kk_ref[...] = inweight * head_key

    def readout(l, p, padded, old_factor, fresh):
        off, count = parts[p]
        acc = jnp.zeros((rows, rows), F32)
        for at in range(off, off + count, GROUP):
            c = mem[l, pl.ds(at, GROUP)].reshape(GROUP * rows, head).astype(BF16)
            r = lax.dot_general(
                c, padded, (((1,), (1,)), ((), ())), preferred_element_type=F32
            ).reshape(GROUP, rows, rows)
            for i in range(GROUP):
                acc = jnp.where(lane == at + i, r[i], acc)
        at = slice(off, off + count)
        gath[2 * l + 1, me, pl.ds(off, count)] = (
            old_factor[at] * acc.T[at] + fresh[at]
        ).astype(BF16)

    def update(l, p):
        off, count = parts[p]

        @pl.loop(0, count // GROUP)
        def _(g):
            at = off + g * GROUP
            v = pltpu.roll(vt_ref[...], lax.rem(rows - at, rows), 1)
            for i in range(GROUP):
                mem[l, at + i] = mem[l, at + i] * decay_ref[pl.ds(at + i, 1), :] + v[
                    :, i : i + 1
                ] * kk_ref[pl.ds(at + i, 1), :]

    def output(l, p):
        g = 2 * l + 1
        at = pl.ds(*parts[p])
        moved = None
        for k in range(-1, len(groups)):
            if k < 0:
                arrived(g, p, 3, 1)
            else:
                arrived(g, p, k, 2 * len(groups[k]))
            for c in [chip] if k < 0 else groups[k]:
                x = jnp.concatenate((gath[g, 2 * c, at], gath[g, 2 * c + 1, at]), axis=1)
                w = wout[l, pl.ds(lanes(c * 2 * rows, 2 * rows), 2 * rows), :]
                part = jnp.dot(x, w, preferred_element_type=F32)
                moved = part if moved is None else moved + part
        old = jnp.concatenate((gath[2 * l, 2 * chip, at], gath[2 * l, 2 * chip + 1, at]), axis=1)
        nxt = (old.astype(F32) + moved).astype(BF16)
        gath[g + 1, 2 * chip, at] = nxt[:, :rows]
        if l + 1 < blocks:
            gath[g + 1, 2 * chip + 1, at] = nxt[:, rows:]
            pair_copy(g + 1, p, chip, 3, gsend.at[g + 1], sibling).start()
            for c, group in targets:
                pair_copy(g + 1, p, chip, group, gsend.at[g + 1], c * 2 + 1).start()
        else:
            block_copy(g + 1, p, 2 * chip, 3, gsend.at[g + 1], sibling).start()
            new_tokens[at] = nxt[:, rows:]

    for l in range(blocks):
        loaded(wgi.at[l], local_sem.at[l, 1])
        wgate[l] = wgi[l].astype(F32).reshape(2 * heads, width).astype(BF16)
        if l == 0:
            sums_send.wait()
        ref = wbig.at[l, :, pl.ds(0, 2 * rows)]
        remote(ref, wsend.at[l, 0], wrecv.at[l, 0], sibling).wait()
        padded, old_factor, fresh, held = project(l)
        loaded(mem.at[l], mem_sem.at[l])
        for p in range(len(parts)):
            readout(l, p, padded, old_factor, fresh)
            send_own(2 * l + 1, p)

            @pl.when(core == 0)
            def _():
                block_copy(2 * l + 1, p, me, 3, gsend.at[2 * l + 1], sibling).start()

        keep(l, held)
        if l + 1 < blocks:
            push_weights(l + 1)
        for p in range(len(parts)):
            update(l, p)

        @pl.when(core == 1)
        def _():
            ref = wout.at[l, :, pl.ds(0, rows)]
            remote(ref, wsend.at[l, 1], wrecv.at[l, 1], sibling).wait_recv()
            for p in range(len(parts)):
                output(l, p)

    flushed(gath.at[0, pl.ds(0, chips)], gsend.at[0])

    @pl.when(core == 0)
    def _():
        for l in range(blocks):
            flushed(gath.at[0, pl.ds(0, chips)], gsend.at[2 * l + 1])
            flushed(wout.at[l, :, pl.ds(0, rows)], wsend.at[l, 1])
        for p in range(len(parts)):
            arrived(2 * blocks, p, 3, 1)
            new_tokens[pl.ds(*parts[p])] = gath[2 * blocks, me, pl.ds(*parts[p])]

    @pl.when(core == 1)
    def _():
        for l in range(blocks):
            flushed(gath.at[0, pl.ds(0, chips - 1)], gsend.at[2 * l + 1])
            flushed(gath.at[0, pl.ds(0, n - 2)], gfwd.at[l])
            flushed(gath.at[0, pl.ds(0, n if l + 1 < blocks else 1)], gsend.at[2 * l + 2])


def from_partner(value, axis, stride):
    mask = 2**stride
    pairs = [(source, source ^ mask) for source in range(lax.axis_size(axis))]
    return lax.ppermute(value, axis, pairs)


def plain_body(
    tokens,
    lengths,
    cell_memory,
    key_sums,
    stabilizer,
    norm_gain,
    query_weight,
    key_weight,
    value_weight,
    outgate_weight,
    ingate_weight,
    forget_weight,
    ingate_bias,
    forget_bias,
    forget_slope,
    head_gain,
    output_weight,
):
    devices = lax.axis_size("tp")
    split_count = devices // HEADS
    own_index = lax.axis_index("tp")
    head_id = own_index // split_count
    onehot = (jnp.arange(HEADS) == head_id).astype(jnp.float32)
    position = lengths.astype(jnp.float32) / MAXLEN
    current = tokens
    memories, sums_list, stabs = ([], [], [])
    for block_id in range(cell_memory.shape[0]):
        gathered_rows = lax.all_gather(current, "tp", axis=1, tiled=True)
        row_float = gathered_rows.astype(jnp.float32)
        normed = (
            row_float
            * lax.rsqrt(jnp.mean(row_float * row_float, axis=-1, keepdims=True) + EPS)
            * norm_gain[block_id].astype(jnp.float32)
        ).astype(jnp.bfloat16)
        queries = jnp.dot(
            normed, query_weight[block_id], preferred_element_type=jnp.float32
        ).astype(jnp.bfloat16)
        key_rows = (
            jnp.dot(normed, key_weight[block_id], preferred_element_type=jnp.float32)
            * HEAD ** (-0.5)
        ).astype(jnp.bfloat16)
        values = jnp.dot(normed, value_weight[block_id], preferred_element_type=jnp.float32).astype(
            jnp.bfloat16
        )
        outgate = jnp.dot(
            normed, outgate_weight[block_id], preferred_element_type=jnp.float32
        ).astype(jnp.bfloat16)
        ingate = (
            jnp.dot(normed, ingate_weight[block_id], preferred_element_type=jnp.float32)
            + ingate_bias[block_id]
        )
        forget = jax.nn.log_sigmoid(
            jnp.dot(normed, forget_weight[block_id], preferred_element_type=jnp.float32)
            + forget_bias[block_id]
            + forget_slope[block_id] * position[:, None]
        )
        stab_new = jnp.maximum(forget + stabilizer[block_id], ingate)
        decays = jnp.exp(forget + stabilizer[block_id] - stab_new)
        in_weight = jnp.exp(ingate - stab_new)
        decay_own = jnp.sum(decays * onehot, axis=1)
        inweight_own = jnp.sum(in_weight * onehot, axis=1)
        sums_new = decay_own[:, None] * key_sums[block_id] + inweight_own[
            :, None
        ] * key_rows.astype(jnp.float32)
        head_pair = jnp.stack((queries, key_rows))
        head_sums = sums_new
        for level in range(split_count.bit_length() - 1):
            partner = from_partner(head_pair, "tp", level)
            upper = own_index // (1 << level) % 2 == 1
            lower_half = jnp.where(upper, partner, head_pair)
            upper_half = jnp.where(upper, head_pair, partner)
            head_pair = jnp.concatenate((lower_half, upper_half), axis=2)
            sums_mate = from_partner(head_sums, "tp", level)
            sums_low = jnp.where(upper, sums_mate, head_sums)
            sums_high = jnp.where(upper, head_sums, sums_mate)
            head_sums = jnp.concatenate((sums_low, sums_high), axis=1)
        head_query = head_pair[0].astype(jnp.float32)
        head_keys = head_pair[1].astype(jnp.float32)
        mem_new = (
            decay_own[:, None, None] * cell_memory[block_id]
            + inweight_own[:, None, None]
            * values.astype(jnp.float32)[:, :, None]
            * head_keys[:, None, :]
        )
        numerator = jnp.einsum("bvk,bk->bv", mem_new, head_query, precision=lax.Precision.HIGHEST)
        denominator = jnp.maximum(jnp.abs(jnp.sum(head_sums * head_query, axis=1)), 1.0)
        hidden = numerator / denominator[:, None]
        gated_out = (
            hidden
            * head_gain[block_id].astype(jnp.float32)
            * jax.nn.sigmoid(outgate.astype(jnp.float32))
        ).astype(jnp.bfloat16)
        out_weight = output_weight[block_id]
        projected = jnp.dot(
            lax.all_gather(gated_out, "tp", axis=1, tiled=True),
            out_weight,
            preferred_element_type=jnp.float32,
        )
        current = (current.astype(jnp.float32) + projected).astype(jnp.bfloat16)
        memories.append(mem_new)
        sums_list.append(sums_new)
        stabs.append(stab_new)
    return (current, jnp.stack(memories), jnp.stack(sums_list), jnp.stack(stabs))


def write_out(*refs):
    sems = refs[8]
    copies = [pltpu.make_async_copy(refs[i], refs[4 + i], sems.at[i]) for i in (0, 2, 3)]
    blocks, batch = refs[1].shape[:2]
    for l in range(blocks):
        for g in range(batch // GROUP):
            at = pl.ds(g * GROUP, GROUP)
            copies.append(
                pltpu.make_async_copy(
                    refs[1].at[l, at], refs[5].at[l, at], sems.at[4 + l * (batch // GROUP) + g]
                )
            )
    for c in copies:
        c.start()
    for c in copies:
        c.wait()


def body(*args):
    tokens, lengths, cell_memory, key_sums, stabilizer = args[:5]
    n = lax.axis_size("tp")
    blocks, batch, rows, head = cell_memory.shape
    heads = stabilizer.shape[2]
    width = args[6].shape[1]
    if n != 2 * heads or n % 8 or blocks < 2 or rows < batch or rows % 128 or batch % 16 or batch < 32:
        return plain_body(*args)
    parts = parts_of(batch)
    vm = pl.BlockSpec(memory_space=pltpu.VMEM)
    anyspace = pl.BlockSpec(memory_space=pl.ANY)
    dma = pltpu.SemaphoreType.DMA
    in_specs = [pl.BlockSpec(memory_space=pltpu.HBM)] * 17
    results = pl.pallas_call(
        functools.partial(kernel, n),
        out_shape=(
            pltpu.VMEM((batch, rows), BF16),
            pltpu.VMEM(cell_memory.shape, F32),
            pltpu.VMEM(key_sums.shape, F32),
            pltpu.VMEM((blocks, heads, batch), F32),
        ),
        in_specs=in_specs,
        out_specs=(vm, vm, vm, vm),
        scratch_shapes=[
            pltpu.VMEM((1, batch), jnp.int32),
            pltpu.VMEM((blocks, heads, batch), F32),
            pltpu.VMEM((blocks, width), BF16),
            pltpu.VMEM((blocks, heads), F32),
            pltpu.VMEM((blocks, heads), F32),
            pltpu.VMEM((blocks, heads), F32),
            pltpu.VMEM((blocks, rows), BF16),
            pltpu.VMEM((blocks, width, 2 * head + 2 * rows), BF16),
            pltpu.VMEM((blocks, width, 2 * rows), BF16),
            pltpu.VMEM((blocks, 2, heads, width), BF16),
            pltpu.VMEM((blocks, 2 * heads, width), BF16),
            dma((7,)),
            pltpu.VMEM((2 * blocks + 1, n, batch, rows), BF16),
            pltpu.VMEM((2, blocks, batch, rows), F32),
            pltpu.VMEM((rows, rows), F32),
            pltpu.VMEM((batch, head), F32),
            pltpu.VMEM((batch, head), F32),
            dma((blocks, 4)),
            dma((blocks,)),
            dma((2 * blocks + 1,)),
            dma((blocks,)),
            dma((2 * blocks + 1, len(parts), 4)),
            dma((blocks, 2)),
            dma((blocks, 2)),
            dma,
            dma,
        ],
        compiler_params=pltpu.CompilerParams(
            collective_id=0, has_side_effects=True, vmem_limit_bytes=45500000
        ),
    )(
        tokens,
        lengths.reshape(1, batch),
        cell_memory,
        key_sums,
        stabilizer.swapaxes(1, 2),
        *args[5:10],
        args[10].swapaxes(1, 2),
        args[11].swapaxes(1, 2),
        *args[12:],
    )
    final = pl.pallas_call(
        write_out,
        out_shape=tuple(jax.ShapeDtypeStruct(r.shape, r.dtype) for r in results),
        in_specs=[anyspace] * 4,
        out_specs=(anyspace,) * 4,
        scratch_shapes=[dma((4 + blocks * (batch // GROUP),))],
        compiler_params=pltpu.CompilerParams(vmem_limit_bytes=1024 * 1024),
    )(*results)
    return (*final[:3], final[3].swapaxes(1, 2))


def solution(mesh):
    in_specs = (
        P("grp", "tp"),
        P("grp"),
        P(None, "grp", "tp", None),
        P(None, "grp", "tp"),
        P(None, "grp", None),
        P(),
        P(None, None, "tp"),
        P(None, None, "tp"),
        P(None, None, "tp"),
        P(None, None, "tp"),
        P(),
        P(),
        P(),
        P(),
        P(),
        P(None, "tp"),
        P(None, None, "tp"),
    )
    out_specs = (
        P("grp", "tp"),
        P(None, "grp", "tp", None),
        P(None, "grp", "tp"),
        P(None, "grp", None),
    )
    return jax.shard_map(body, mesh=mesh, in_specs=in_specs, out_specs=out_specs, check_vma=False)
```

profile of v0, /device:TPU:0, one launch (start us, length us, event | category | flops | bytes accessed | tf_op | source)
XLA Modules:
  0.0 40.8 jit_solution(9056657304750750944)
XLA Ops:
  0.6 32.8 %shard_map.192 = (bf16[80,128]{1,0:T(8,128)(2,1)S(1)}, f32[2,80,128,256]{3,2,1,0:T(8,128)S(1)}, f32[2,80,128]{2,1,0:T(8,128)S(1)}, f32[2,8,80]{2,1,0:T(8,128)S(1)}) custom-call(bf16[80,128]{1,0:T(8,128)(2,1)} %tokens.1, s32[1,80]{1,0:T(1,128)} %bitcast.8, f32[2,80,128,256]{3,2,1,0:T(8,128)} %cell_memory.1, f32[2,80,128]{2,1,0:T(8,128)} %key_sums.1, ...), custom_call_target="tpu_custom_call" | custom-call | tf_op jit(solution)/shard_map/pallas_call | solution.py:550
  33.5 7.3 %shard_map.193 = (bf16[80,128]{1,0:T(8,128)(2,1)}, f32[2,80,128,256]{3,2,1,0:T(8,128)}, f32[2,80,128]{2,1,0:T(8,128)}, f32[2,8,80]{2,1,0:T(8,128)}) custom-call(bf16[80,128]{1,0:T(8,128)(2,1)S(1)} %get-tuple-element.12.refs_0_, f32[2,80,128,256]{3,2,1,0:T(8,128)S(1)} %get-tuple-element.13.refs_1_, f32[2,80,128]{2,1,0:T(8,128)S(1)} %get-tuple-element.14.refs_2_, ...), custom_call_target="tpu_custom_call" | custom-call | tf_op jit(solution)/shard_map/pallas_call | solution.py:602
where the time goes:
time: 40.9 us; the launch traced here: 40.8 us
  Pallas kernels  40.1 us (98%)
  between operations  0.65 us (2%)
    pallas_call x1, Pallas kernels, body(): pl.pallas_call(functools.partial(kernel, n), out_shape=(pltpu.VMEM((batch...  32.8 us
    pallas_call x1, Pallas kernels, body(): pl.pallas_call(write_out, out_shape=tuple((jax.ShapeDtypeStruct(r.shape,...  7.33 us

commit v1 on v0

--- a/solution.py
+++ b/solution.py
@@ -15,11 +15,13 @@
 F32 = jnp.float32
 BF16 = jnp.bfloat16
 GROUP = 8
+FOLD = 16
 
 
 def parts_of(batch):
-    first = (batch + 31) // 32 * 16
-    return ((0, first), (first, batch - first))
+    first = 16
+    middle = first + (batch - first) // 32 * 16
+    return ((0, first), (first, middle - first), (middle, batch - middle))
 
 
 def kernel(
@@ -62,6 +64,8 @@
     vt_ref,
     decay_ref,
     kk_ref,
+    q_ref,
+    picks,
     local_sem,
     mem_sem,
     gsend,
@@ -236,6 +240,12 @@
         jnp.where(eye, lengths_in[...].astype(F32) / MAXLEN, 0.0), axis=1, keepdims=True
     )
     lane = lax.broadcasted_iota(jnp.int32, (rows, rows), 1)
+
+    @pl.loop(0, batch)
+    def _(b):
+        at = pl.ds(lanes(b * rows, rows), rows)
+        picks[at] = jnp.where(lane == b, 1.0, 0.0).astype(BF16)
+
     head_mask = lax.broadcasted_iota(jnp.int32, (batch, heads), 1) == own_head
 
     def project(l):
@@ -283,9 +293,9 @@
         old = jnp.concatenate((sums[0, l], sums[1, l]), axis=1)
         sum_dot = jnp.sum(old * query_float, axis=1, keepdims=True)
         denominator = jnp.maximum(jnp.abs(decay * sum_dot + inweight * key_dot), 1.0)
-        padded = jnp.concatenate((head_query, jnp.zeros((rows - batch, head), BF16)), axis=0)
         factor = gate / denominator
-        return padded, decay * factor, inweight * key_dot * value * factor, (
+        q_ref[...] = query_float
+        return decay * factor, inweight * key_dot * value * factor, (
             stab,
             decay,
             inweight,
@@ -302,16 +312,19 @@
         decay_ref[...] = jnp.broadcast_to(decay, (batch, head))
         kk_ref[...] = inweight * head_key
 
-    def readout(l, p, padded, old_factor, fresh):
+    def readout(l, p, old_factor, fresh):
         off, count = parts[p]
         acc = jnp.zeros((rows, rows), F32)
-        for at in range(off, off + count, GROUP):
-            c = mem[l, pl.ds(at, GROUP)].reshape(GROUP * rows, head).astype(BF16)
-            r = lax.dot_general(
-                c, padded, (((1,), (1,)), ((), ())), preferred_element_type=F32
-            ).reshape(GROUP, rows, rows)
-            for i in range(GROUP):
-                acc = jnp.where(lane == at + i, r[i], acc)
+        for at in range(off, off + count, FOLD):
+            folded = []
+            for b in range(at, at + FOLD):
+                product = mem[l, b] * q_ref[pl.ds(b, 1), :]
+                folded.append((product[:, :rows] + product[:, rows:]).astype(BF16))
+            acc = acc + jnp.dot(
+                jnp.concatenate(folded, axis=1),
+                picks[pl.ds(at * rows, FOLD * rows), :],
+                preferred_element_type=F32,
+            )
         at = slice(off, off + count)
         gath[2 * l + 1, me, pl.ds(off, count)] = (
             old_factor[at] * acc.T[at] + fresh[at]
@@ -362,10 +375,10 @@
             sums_send.wait()
         ref = wbig.at[l, :, pl.ds(0, 2 * rows)]
         remote(ref, wsend.at[l, 0], wrecv.at[l, 0], sibling).wait()
-        padded, old_factor, fresh, held = project(l)
         loaded(mem.at[l], mem_sem.at[l])
+        old_factor, fresh, held = project(l)
         for p in range(len(parts)):
-            readout(l, p, padded, old_factor, fresh)
+            readout(l, p, old_factor, fresh)
             send_own(2 * l + 1, p)
 
             @pl.when(core == 0)
@@ -540,7 +553,7 @@
     blocks, batch, rows, head = cell_memory.shape
     heads = stabilizer.shape[2]
     width = args[6].shape[1]
-    if n != 2 * heads or n % 8 or blocks < 2 or rows < batch or rows % 128 or batch % 16 or batch < 32:
+    if n != 2 * heads or n % 8 or blocks < 2 or rows < batch or rows % 128 or batch % 16 or batch < 48:
         return plain_body(*args)
     parts = parts_of(batch)
     vm = pl.BlockSpec(memory_space=pltpu.VMEM)
@@ -575,6 +588,8 @@
             pltpu.VMEM((rows, rows), F32),
             pltpu.VMEM((batch, head), F32),
             pltpu.VMEM((batch, head), F32),
+            pltpu.VMEM((batch, head), F32),
+            pltpu.VMEM((batch * rows, rows), BF16),
             dma((blocks, 4)),
             dma((blocks,)),
             dma((2 * blocks + 1,)),

time: 40.9 us -> 39.2 us (0.958)
  Pallas kernels: 40.1 us -> 38.4 us
    pallas_call x1, Pallas kernels: 32.8 us -> 31 us  [body(): pl.pallas_call(functools.partial(kernel, n), out_shape=(pltpu.VMEM((batch...]
where the time goes in v1:
time: 39.2 us; the launch traced here: 39 us
  Pallas kernels  38.4 us (98%)
  between operations  0.65 us (2%)
    pallas_call x1, Pallas kernels, body(): pl.pallas_call(functools.partial(kernel, n), out_shape=(pltpu.VMEM((batch...  31 us
    pallas_call x1, Pallas kernels, body(): pl.pallas_call(write_out, out_shape=tuple((jax.ShapeDtypeStruct(r.shape,...  7.33 us

profile of v1, /device:TPU:0, one launch (start us, length us, event | category | flops | bytes accessed | tf_op | source)
XLA Modules:
  0.0 39.0 jit_solution(7987022300568500548)
XLA Ops:
  0.6 31.0 %shard_map.192 = (bf16[80,128]{1,0:T(8,128)(2,1)S(1)}, f32[2,80,128,256]{3,2,1,0:T(8,128)S(1)}, f32[2,80,128]{2,1,0:T(8,128)S(1)}, f32[2,8,80]{2,1,0:T(8,128)S(1)}) custom-call(bf16[80,128]{1,0:T(8,128)(2,1)} %tokens.1, s32[1,80]{1,0:T(1,128)} %bitcast.8, f32[2,80,128,256]{3,2,1,0:T(8,128)} %cell_memory.1, f32[2,80,128]{2,1,0:T(8,128)} %key_sums.1, ...), custom_call_target="tpu_custom_call" | custom-call | tf_op jit(solution)/shard_map/pallas_call | solution.py:563
  31.7 7.3 %shard_map.193 = (bf16[80,128]{1,0:T(8,128)(2,1)}, f32[2,80,128,256]{3,2,1,0:T(8,128)}, f32[2,80,128]{2,1,0:T(8,128)}, f32[2,8,80]{2,1,0:T(8,128)}) custom-call(bf16[80,128]{1,0:T(8,128)(2,1)S(1)} %get-tuple-element.12.refs_0_, f32[2,80,128,256]{3,2,1,0:T(8,128)S(1)} %get-tuple-element.13.refs_1_, f32[2,80,128]{2,1,0:T(8,128)S(1)} %get-tuple-element.14.refs_2_, ...), custom_call_target="tpu_custom_call" | custom-call | tf_op jit(solution)/shard_map/pallas_call | solution.py:617

commit v2 on v1

--- a/solution.py
+++ b/solution.py
@@ -19,9 +19,7 @@
 
 
 def parts_of(batch):
-    first = 16
-    middle = first + (batch - first) // 32 * 16
-    return ((0, first), (first, middle - first), (middle, batch - middle))
+    return ((0, 16), (16, 16), (32, batch - 32))
 
 
 def kernel(
@@ -168,22 +166,30 @@
             device_id_type=MESH,
         )
 
+    last = len(parts) - 1
+
+    def signal(g, p, group):
+        if p < last:
+            return grecv.at[g, 2 * p + (group == 3)]
+        return grecv.at[g, 2 * last + group]
+
     def block_copy(g, p, slot, group, send, dest):
-        return remote(gath.at[g, slot, pl.ds(*parts[p])], send, grecv.at[g, p, group], dest)
+        return remote(gath.at[g, slot, pl.ds(*parts[p])], send, signal(g, p, group), dest)
 
     def pair_copy(g, p, c, group, send, dest):
         ref = gath.at[g, pl.ds(2 * c, 2), pl.ds(*parts[p])]
-        return remote(ref, send, grecv.at[g, p, group], dest)
+        return remote(ref, send, signal(g, p, group), dest)
 
     def arrived(g, p, group, count):
         ref = gath.at[g, pl.ds(0, count), pl.ds(*parts[p])]
-        remote(ref, gsend.at[g], grecv.at[g, p, group], sibling).wait_recv()
+        remote(ref, gsend.at[g], signal(g, p, group), sibling).wait_recv()
 
     def flushed(ref, sem):
         remote(ref, sem, wrecv.at[0, 0], sibling).wait_send()
 
     def send_own(g, p):
         for c, group in targets:
+            group = group if p == last else 0
             block_copy(g, p, me, group, gsend.at[g], c * 2 + 1).start()
 
     def gathered(l, k):
@@ -200,11 +206,14 @@
 
             return [chip]
         for p in range(len(parts)):
-            arrived(g, p, k, 2 * len(groups[k]))
+            if p < last and k > 0:
+                continue
+            here = groups[k] if p == last else sum(groups, [])
+            arrived(g, p, k, 2 * len(here))
 
             @pl.when(core == 1)
             def _():
-                for c in groups[k]:
+                for c in here:
                     pair_copy(g, p, c, k, gfwd.at[l], sibling).start()
 
         return groups[k]
@@ -349,8 +358,10 @@
         for k in range(-1, len(groups)):
             if k < 0:
                 arrived(g, p, 3, 1)
-            else:
+            elif p == last:
                 arrived(g, p, k, 2 * len(groups[k]))
+            elif k == 0:
+                arrived(g, p, k, n - 2)
             for c in [chip] if k < 0 else groups[k]:
                 x = jnp.concatenate((gath[g, 2 * c, at], gath[g, 2 * c + 1, at]), axis=1)
                 w = wout[l, pl.ds(lanes(c * 2 * rows, 2 * rows), 2 * rows), :]
@@ -363,6 +374,7 @@
             gath[g + 1, 2 * chip + 1, at] = nxt[:, rows:]
             pair_copy(g + 1, p, chip, 3, gsend.at[g + 1], sibling).start()
             for c, group in targets:
+                group = group if p == last else 0
                 pair_copy(g + 1, p, chip, group, gsend.at[g + 1], c * 2 + 1).start()
         else:
             block_copy(g + 1, p, 2 * chip, 3, gsend.at[g + 1], sibling).start()
@@ -594,7 +606,7 @@
             dma((blocks,)),
             dma((2 * blocks + 1,)),
             dma((blocks,)),
-            dma((2 * blocks + 1, len(parts), 4)),
+            dma((2 * blocks + 1, 2 * len(parts) + 2)),
             dma((blocks, 2)),
             dma((blocks, 2)),
             dma,

time: 39.2 us -> 38.9 us (level)
  no operation moved by 1% of the time
where the time goes in v2:
time: 38.9 us; the launch traced here: 38.8 us
  Pallas kernels  38.1 us (98%)
  between operations  0.65 us (2%)
    pallas_call x1, Pallas kernels, body(): pl.pallas_call(functools.partial(kernel, n), out_shape=(pltpu.VMEM((batch...  30.8 us
    pallas_call x1, Pallas kernels, body(): pl.pallas_call(write_out, out_shape=tuple((jax.ShapeDtypeStruct(r.shape,...  7.33 us

profile of v2, /device:TPU:0, one launch (start us, length us, event | category | flops | bytes accessed | tf_op | source)
XLA Modules:
  0.0 38.8 jit_solution(1657661592727942025)
XLA Ops:
  0.6 30.8 %shard_map.192 = (bf16[80,128]{1,0:T(8,128)(2,1)S(1)}, f32[2,80,128,256]{3,2,1,0:T(8,128)S(1)}, f32[2,80,128]{2,1,0:T(8,128)S(1)}, f32[2,8,80]{2,1,0:T(8,128)S(1)}) custom-call(bf16[80,128]{1,0:T(8,128)(2,1)} %tokens.1, s32[1,80]{1,0:T(1,128)} %bitcast.8, f32[2,80,128,256]{3,2,1,0:T(8,128)} %cell_memory.1, f32[2,80,128]{2,1,0:T(8,128)} %key_sums.1, ...), custom_call_target="tpu_custom_call" | custom-call | tf_op jit(solution)/shard_map/pallas_call | solution.py:575
  31.4 7.3 %shard_map.193 = (bf16[80,128]{1,0:T(8,128)(2,1)}, f32[2,80,128,256]{3,2,1,0:T(8,128)}, f32[2,80,128]{2,1,0:T(8,128)}, f32[2,8,80]{2,1,0:T(8,128)}) custom-call(bf16[80,128]{1,0:T(8,128)(2,1)S(1)} %get-tuple-element.12.refs_0_, f32[2,80,128,256]{3,2,1,0:T(8,128)S(1)} %get-tuple-element.13.refs_1_, f32[2,80,128]{2,1,0:T(8,128)S(1)} %get-tuple-element.14.refs_2_, ...), custom_call_target="tpu_custom_call" | custom-call | tf_op jit(solution)/shard_map/pallas_call | solution.py:629
